TPU v7x, 32 devices: a whole 2x2x4 slice. The times are simulated.
32 devices in a mesh: ep: 8 (over z, core), tp: 4 (over y, x).
Axes of the slice: x: 2, y: 2, z: 4, core: 2. Of those that a mesh axis runs over, the one named last changes fastest.
Arguments:
- tokens: bfloat16 [1536, 4096], P('ep'), may hold values from -6 to 6
- expert_ids: int32 [1536, 2], P('ep'), may hold values from 0 to 7, all different within a row; in each aligned block of 192 rows (0 to 191, 192 to 383, ...) at most 60 rows name the same one
- route_weight: float32 [1536, 2], P('ep'), may hold values from 0.1 to 1
- norm_gain: float32 [4096], replicated, may hold values from 0.1 to 1.9
- gate_weight: bfloat16 [8, 4096, 4096], P('ep', None, 'tp'), may hold values from -0.28125 to 0.28125
- up_weight: bfloat16 [8, 4096, 4096], P('ep', None, 'tp'), may hold values from -0.28125 to 0.28125
- down_weight: bfloat16 [8, 4096, 4096], P('ep', None, 'tp'), may hold values from -0.028076172 to 0.028076172
Outputs:
- mixed: bfloat16 [1536, 4096], P('ep', 'tp')
Inputs may be any that keep to these rules, and one draw needn't show every extreme that they name: `expert_ids`: each row names 2 different experts. In each aligned block of 192 rows (the tokens of one index of ep) no expert is named by more than 60 rows, and in some block some expert is named by exactly 60 rows.
All inputs are finite; a program needn't handle non-finite values.
Results may differ from a plain program's by a relative error of at most 0.007.
Values may be sent and summed in bfloat16 or wider, within the bound.
A program may use at most 64 MiB of HBM per device.

v0:
```python
import jax
import jax.numpy as jnp
from jax import lax
from jax.sharding import PartitionSpec as P

EPS = 1e-06
LIMIT = 7.0
ALPHA = 1.702


def rms_norm(tokens, norm_gain):
    values = tokens.astype(jnp.float32)
    scale = lax.rsqrt(jnp.mean(values * values, axis=-1, keepdims=True) + EPS)
    return (values * scale * norm_gain).astype(jnp.bfloat16)


def clamped_unit(gate_pre, up_pre):
    gate = jnp.minimum(gate_pre, LIMIT)
    up_part = jnp.clip(up_pre, -LIMIT, LIMIT)
    return ((up_part + 1.0) * gate * jax.nn.sigmoid(ALPHA * gate)).astype(jnp.bfloat16)


def slot_numbers(id_blocks, experts, capacity):
    onehot = (id_blocks[:, :, None] == jnp.arange(experts, dtype=jnp.int32)[None, None, :]).astype(
        jnp.int32
    )
    before = jnp.cumsum(onehot, axis=1) - onehot
    position = jnp.sum(before * onehot, axis=2)
    return id_blocks * capacity + position


def project_down(hidden, down_weight):
    result = jnp.einsum(
        "sejf,efd->sejd",
        lax.all_gather(hidden, "tp", axis=3, tiled=True),
        down_weight,
        preferred_element_type=jnp.float32,
    )
    return result.astype(jnp.bfloat16)


def on_device(tokens, expert_ids, route_weight, norm_gain, gate_weight, up_weight, down_weight):
    n_ep = lax.axis_size("ep")
    n_tp = lax.axis_size("tp")
    tok_rows, width = tokens.shape
    top = expert_ids.shape[1]
    local_experts = gate_weight.shape[0]
    experts = local_experts * n_ep
    capacity = 5 * tok_rows * top // (4 * experts)
    cols = width // n_tp
    normed = rms_norm(tokens, norm_gain)
    dest = slot_numbers(expert_ids.reshape(1, tok_rows * top), experts, capacity).reshape(-1)
    slot_range = jnp.arange(experts * capacity, dtype=jnp.int32)
    match = slot_range[:, None] == dest[None, :]
    pick = jnp.any(match.reshape(experts * capacity, tok_rows, top), axis=2).astype(jnp.bfloat16)
    own = lax.dynamic_slice_in_dim(normed, lax.axis_index("tp") * cols, cols, 1)
    buffer = jnp.dot(pick, own, preferred_element_type=jnp.float32).astype(jnp.bfloat16)
    buffer = buffer.reshape(n_ep, local_experts, capacity, cols)
    arrived = lax.all_to_all(buffer, "ep", split_axis=0, concat_axis=0, tiled=True)
    piece = lax.all_gather(arrived, "tp", axis=3, tiled=True)
    gate_part = jnp.einsum("sejd,edf->sejf", piece, gate_weight, preferred_element_type=jnp.float32)
    up_part = jnp.einsum("sejd,edf->sejf", piece, up_weight, preferred_element_type=jnp.float32)
    hidden = clamped_unit(gate_part, up_part)
    result = project_down(hidden, down_weight)
    back = lax.all_to_all(result, "ep", split_axis=0, concat_axis=0, tiled=True).reshape(
        experts * capacity, cols
    )
    chosen = jnp.transpose(match).astype(jnp.bfloat16)
    per_copy = jnp.dot(chosen, back, preferred_element_type=jnp.float32).reshape(
        tok_rows, top, cols
    )
    mixed = jnp.sum(per_copy * route_weight[:, :, None], axis=1)
    return mixed.astype(jnp.bfloat16)


def solution(mesh):
    placed = (
        P("ep", None),
        P("ep", None),
        P("ep", None),
        P(),
        P("ep", None, "tp"),
        P("ep", None, "tp"),
        P("ep", None, "tp"),
    )
    return jax.shard_map(
        on_device, mesh=mesh, in_specs=placed, out_specs=P("ep", "tp"), check_vma=False
    )
```

profile of v0, /device:TPU:0, one launch (start us, length us, event | category | flops | bytes accessed | tf_op | source)
XLA Modules:
  0.0 220.5 jit_solution(3522461065963199480)
XLA Ops:
  6.5 3.5 %convert_element_type.41 = f32[192,4096]{1,0:T(8,128)} convert(bf16[192,4096]{1,0:T(8,128)(2,1)} %param.7) | non-fusion elementwise | flops 786432 | bytes 4718592 | tf_op jit(solution)/shard_map/convert_element_type | solution.py:12
  10.1 0.4 multiply_reduce_fusion
  10.5 0.1 copy.28
  10.6 0.1 reshape.211
  10.8 0.9 reduce-window.6
  11.6 0.2 slice_reduce_fusion
  11.9 0.1 fusion.36
  12.0 0.1 reduce_sum.30
  12.2 0.2 fusion.30
  12.4 0.7 dynamic-slice
  13.1 1.6 convolution_convert_fusion
  14.8 0.2 reshape.217
  14.9 32.8 %all_to_all.10 = bf16[8,1,60,1024]{3,2,1,0:T(8,128)(2,1)} all-to-all(bf16[8,1,60,1024]{3,2,1,0:T(8,128)(2,1)S(1)} %bitcast.73), channel_id=1, replica_groups=mesh['ep'=8,'tp'=4] {'ep'}, dimensions={0} | all-to-all | bytes 1966080 | tf_op jit(solution)/shard_map/all_to_all | solution.py:59
  47.8 51.6 %all-gather.3.cloned.1.call-done = bf16[8,1,60,4096]{3,2,0,1:T(8,128)(2,1)} async-done(((bf16[8,1,60,1024]{3,2,0,1:T(8,128)(2,1)}), bf16[8,1,60,4096]{3,2,0,1:T(8,128)(2,1)}) %all-gather.3.cloned.1.call-update) | async-done | bytes 3932176 | tf_op jit(solution)/shard_map/all_gather | solution.py:60
  99.4 9.1 %fusion.2 = f32[8,60,1024]{2,1,0:T(8,128)S(1)} fusion(bf16[1,4096,1024]{2,1,0:T(8,128)(2,1)} %param.11, bf16[8,1,60,4096]{3,2,0,1:T(8,128)(2,1)} %all-gather.3.cloned.1.call-done), kind=kOutput, calls=%fused_computation.2 | convolution fusion | flops 4026531840 | bytes 14286848 | tf_op jit(solution)/shard_map/sejd,edf->sejf/dot_general | solution.py:61
  108.6 9.4 %fusion.23 = bf16[8,1,60,1024]{3,2,0,1:T(8,128)(2,1)} fusion(f32[8,60,1024]{2,1,0:T(8,128)S(1)} %fusion.2, bf16[1,4096,1024]{2,1,0:T(8,128)(2,1)} %param.12, bf16[8,1,60,4096]{3,2,0,1:T(8,128)(2,1)S(1)} %copy-done.2), kind=kOutput, calls=%fused_computation.15 | convolution fusion | flops 4031447040 | bytes 15269888 | tf_op jit(solution)/shard_map/sejd,edf->sejf/dot_general | solution.py:62
  118.0 52.7 %all-gather.5.cloned.1.call-done = bf16[8,1,60,4096]{3,2,0,1:T(8,128)(2,1)} async-done(((bf16[8,1,60,1024]{3,2,0,1:T(8,128)(2,1)}), bf16[8,1,60,4096]{3,2,0,1:T(8,128)(2,1)}) %all-gather.5.cloned.1.call-update) | async-done | bytes 3932176 | tf_op jit(solution)/shard_map/all_gather | solution.py:35
  170.7 10.1 %fusion.18 = bf16[8,1,60,1024]{3,2,1,0:T(8,128)(2,1)} fusion(bf16[1,4096,1024]{2,1,0:T(8,128)(2,1)} %param.13, bf16[8,1,60,4096]{3,2,0,1:T(8,128)(2,1)} %all-gather.5.cloned.1.call-done), kind=kOutput, calls=%fused_computation.14 | convolution fusion | flops 4027023360 | bytes 13303808 | tf_op jit(solution)/shard_map/sejf,efd->sejd/dot_general | solution.py:33
  180.8 4.7 %all-to-all-start.1 = ((bf16[8,1,60,1024]{3,2,1,0:T(8,128)(2,1)}), bf16[8,1,60,1024]{3,2,1,0:T(8,128)(2,1)S(1)}, u32[]{:S(2)}, u32[]{:S(2)}) async-start(bf16[8,1,60,1024]{3,2,1,0:T(8,128)(2,1)} %fusion.18), calls=%async_computation.1 | async-start | bytes 2097152 | tf_op jit(solution)/shard_map/all_to_all | solution.py:65
  185.6 0.2 iota_compare_fusion.1
  185.8 0.3 eq.60
  186.0 26.1 %all-to-all-done.1 = bf16[8,1,60,1024]{3,2,1,0:T(8,128)(2,1)S(1)} async-done(((bf16[8,1,60,1024]{3,2,1,0:T(8,128)(2,1)}), bf16[8,1,60,1024]{3,2,1,0:T(8,128)(2,1)S(1)}, u32[]{:S(2)}, u32[]{:S(2)}) %all-to-all-start.1) | async-done | bytes 983072 | tf_op jit(solution)/shard_map/all_to_all | solution.py:65
  212.1 0.2 reshape.235
  212.3 1.4 multiply_reduce_fusion.1
  (21 shorter events, 0.2 us)
Async XLA Ops:
  6.5 3.6 %copy-start = (bf16[192,4096]{1,0:T(8,128)(2,1)S(1)}, bf16[192,4096]{1,0:T(8,128)(2,1)}, u32[]{:S(2)}) copy-start(bf16[192,4096]{1,0:T(8,128)(2,1)} %param.7) | copy-start | bytes 4718596
  6.5 92.9 %all-gather.3.cloned.1.call-start = ((), (), s32[]{:S(2)}) async-start(), calls=%async_computation.2 | async-start | bytes 5242880 | tf_op jit(solution)/shard_map/all_gather | solution.py:60
  6.5 4.0 %copy-start.1 = (s32[192,2]{0,1:T(2,128)S(1)}, s32[192,2]{0,1:T(2,128)}, u32[]{:S(2)}) copy-start(s32[192,2]{0,1:T(2,128)} %param.8) | copy-start | bytes 4612
  47.8 122.9 %all-gather.5.cloned.1.call-start = ((), (), s32[]{:S(2)}) async-start(), calls=%async_computation.3 | async-start | bytes 5242880 | tf_op jit(solution)/shard_map/all_gather | solution.py:35
  99.4 9.1 %copy-start.2 = (bf16[8,1,60,4096]{3,2,0,1:T(8,128)(2,1)S(1)}, bf16[8,1,60,4096]{3,2,0,1:T(8,128)(2,1)}, u32[]{:S(2)}) copy-start(bf16[8,1,60,4096]{3,2,0,1:T(8,128)(2,1)} %all-gather.3.cloned.1.call-done) | copy-start | bytes 11796484
  180.8 31.5 %copy-start.3 = (f32[192,2]{0,1:T(2,128)S(1)}, f32[192,2]{0,1:T(2,128)}, u32[]{:S(2)}) copy-start(f32[192,2]{0,1:T(2,128)} %param.9) | copy-start | bytes 4612
  180.8 31.3 %all-to-all-start.1 = ((bf16[8,1,60,1024]{3,2,1,0:T(8,128)(2,1)}), bf16[8,1,60,1024]{3,2,1,0:T(8,128)(2,1)S(1)}, u32[]{:S(2)}, u32[]{:S(2)}) async-start(bf16[8,1,60,1024]{3,2,1,0:T(8,128)(2,1)} %fusion.18), calls=%async_computation.1 | async-start | bytes 2097152 | tf_op jit(solution)/shard_map/all_to_all | solution.py:65
Sparse Core Ops, SparseCore 0:
  47.9 51.4 all-gather.2
  118.1 52.5 all-gather.4
where the time goes:
time: 221 us
  waiting for transfers between devices  130 us (59%)
  blocking collectives  32.8 us (15%)
  matrix products  31.6 us (14%)
  between operations  13.5 us (6%)
  other arithmetic  5.26 us (2%)
  starting transfers between devices  4.78 us (2%)
    all_gather x1, waiting for transfers between devices, project_down(): lax.all_gather(hidden, 'tp', axis=3, tiled=True)  52.7 us
    all_gather x1, waiting for transfers between devices, on_device(): piece = lax.all_gather(arrived, 'tp', axis=3, tiled=True)  51.6 us
    all_to_all x1, blocking collectives, on_device(): lax.all_to_all(buffer, 'ep', split_axis=0, concat_axis=0, tiled=True)  32.8 us
    all_to_all x1, waiting for transfers between devices, on_device(): lax.all_to_all(result, 'ep', split_axis=0, concat_axis=0, tiled=True)  26.1 us
    dot_general x1, matrix products, project_down(): jnp.einsum('sejf,efd->sejd', lax.all_gather(hidden, 'tp', axis=3, tiled=T...  10.1 us
    dot_general x1, matrix products, on_device(): jnp.einsum('sejd,edf->sejf', piece, up_weight, preferred_element_type=jnp...  9.37 us
    dot_general x1, matrix products, on_device(): jnp.einsum('sejd,edf->sejf', piece, gate_weight, preferred_element_type=j...  9.13 us
    all_to_all x1, starting transfers between devices, on_device(): lax.all_to_all(result, 'ep', split_axis=0, concat_axis=0, tiled=True)  4.74 us
  transfers between devices with their start and end apart: 3, of which 3 were waited for; matrix products, arithmetic and copies ran while one was open for 0% of the time, Pallas kernels for 0%

commit v1 on v0

--- a/solution.py
+++ b/solution.py
@@ -6,6 +6,18 @@
 EPS = 1e-06
 LIMIT = 7.0
 ALPHA = 1.702
+
+
+def summed_around(x, axis, dim, product):
+    size, index, width = (lax.axis_size(axis), lax.axis_index(axis), x.shape[dim])
+    upward = [(i, (i + 1) % size) for i in range(size)]
+    held, total = (x, None)
+    for lap in range(size):
+        coming = lax.ppermute(held, axis, upward) if lap < size - 1 else None
+        absorb = product(held, (index - lap) % size * width)
+        total = absorb if total is None else total + absorb
+        held = coming
+    return total
 
 
 def rms_norm(tokens, norm_gain):
@@ -30,11 +42,16 @@
 
 
 def project_down(hidden, down_weight):
-    result = jnp.einsum(
-        "sejf,efd->sejd",
-        lax.all_gather(hidden, "tp", axis=3, tiled=True),
-        down_weight,
-        preferred_element_type=jnp.float32,
+    result = summed_around(
+        hidden,
+        "tp",
+        3,
+        lambda part, offset: jnp.einsum(
+            "sejf,efd->sejd",
+            part,
+            lax.dynamic_slice_in_dim(down_weight, offset, part.shape[3], axis=1),
+            preferred_element_type=jnp.float32,
+        ),
     )
     return result.astype(jnp.bfloat16)
 

time: 221 us -> 229 us (1.036)
  waiting for transfers between devices: 130 us -> 138 us
    ppermute x0 -> x3, waiting for transfers between devices: none -> 60.5 us  [summed_around(): coming = lax.ppermute(held, axis, upward) if lap < size - 1 else None]
    all_gather x1 -> x0, waiting for transfers between devices: 52.7 us -> none  [project_down(): lax.all_gather(hidden, 'tp', axis=3, tiled=True)]
    dot_general x1 -> x4, matrix products: 10.1 us -> 9.88 us  [project_down(): jnp.einsum('sejf,efd->sejd', part, lax.dynamic_slice_in_dim(down_weight,...]
  transfers between devices with their start and end apart: 3 -> 5, of which waited for: 3 -> 5; matrix products, arithmetic and copies ran while one was open for 0% -> 3% of each run, Pallas kernels for 0% -> 0%
where the time goes in v1:
time: 229 us
  waiting for transfers between devices  138 us (60%)
  blocking collectives  32.8 us (14%)
  matrix products  30.2 us (13%)
  between operations  13.6 us (6%)
  starting transfers between devices  6.84 us (3%)
  local copies, waits for them, and re-layouts  3.75 us (2%)
  other arithmetic  3.58 us (2%)
    ppermute x3, waiting for transfers between devices, summed_around(): coming = lax.ppermute(held, axis, upward) if lap < size - 1 else None  60.5 us
    all_gather x1, waiting for transfers between devices, on_device(): piece = lax.all_gather(arrived, 'tp', axis=3, tiled=True)  51.7 us
    all_to_all x1, blocking collectives, on_device(): lax.all_to_all(buffer, 'ep', split_axis=0, concat_axis=0, tiled=True)  32.8 us
    all_to_all x1, waiting for transfers between devices, on_device(): lax.all_to_all(result, 'ep', split_axis=0, concat_axis=0, tiled=True)  26.1 us
    dot_general x4, matrix products, project_down(): jnp.einsum('sejf,efd->sejd', part, lax.dynamic_slice_in_dim(down_weight,...  9.88 us
    dot_general x1, matrix products, on_device(): jnp.einsum('sejd,edf->sejf', piece, gate_weight, preferred_element_type=j...  9.13 us
    dot_general x1, matrix products, on_device(): jnp.einsum('sejd,edf->sejf', piece, up_weight, preferred_element_type=jnp...  8.38 us
    all_to_all x1, starting transfers between devices, on_device(): lax.all_to_all(result, 'ep', split_axis=0, concat_axis=0, tiled=True)  4.75 us
  transfers between devices with their start and end apart: 5, of which 5 were waited for; matrix products, arithmetic and copies ran while one was open for 3% of the time, Pallas kernels for 0%

profile of v1, /device:TPU:0, one launch (start us, length us, event | category | flops | bytes accessed | tf_op | source)
XLA Modules:
  0.0 229.2 jit_solution(7607586606837907222)
XLA Ops:
  6.5 1.9 convert_element_type.33
  8.4 0.4 multiply_reduce_fusion
  9.1 0.9 reduce-window.6
  10.7 0.7 dynamic-slice
  11.4 1.5 convolution_convert_fusion
  12.9 1.3 reshape.242
  14.3 32.8 %all_to_all.10 = bf16[8,1,60,1024]{3,2,1,0:T(8,128)(2,1)} all-to-all(bf16[8,1,60,1024]{3,2,1,0:T(8,128)(2,1)S(1)} %bitcast.81), channel_id=1, replica_groups=mesh['ep'=8,'tp'=4] {'ep'}, dimensions={0} | all-to-all | bytes 1966080 | tf_op jit(solution)/shard_map/all_to_all | solution.py:76
  47.1 51.7 %all-gather.2.cloned.1.call-done = bf16[8,1,60,4096]{3,2,0,1:T(8,128)(2,1)} async-done(((bf16[8,1,60,1024]{3,2,0,1:T(8,128)(2,1)}), bf16[8,1,60,4096]{3,2,0,1:T(8,128)(2,1)}) %all-gather.2.cloned.1.call-update) | async-done | bytes 3932176 | tf_op jit(solution)/shard_map/all_gather | solution.py:77
  98.8 9.1 %fusion = f32[8,60,1024]{2,1,0:T(8,128)S(1)} fusion(bf16[1,4096,1024]{2,1,0:T(8,128)(2,1)} %param.11, bf16[8,1,60,4096]{3,2,0,1:T(8,128)(2,1)} %all-gather.2.cloned.1.call-done), kind=kOutput, calls=%fused_computation | convolution fusion | flops 4026531840 | bytes 14286848 | tf_op jit(solution)/shard_map/sejd,edf->sejf/dot_general | solution.py:78
  107.9 8.4 %multiply_convert_fusion = bf16[8,60,1024]{2,1,0:T(8,128)(2,1)S(1)} fusion(f32[8,60,1024]{2,1,0:T(8,128)S(1)} %fusion, bf16[1,4096,1024]{2,1,0:T(8,128)(2,1)} %param.12, bf16[8,1,60,4096]{3,2,0,1:T(8,128)(2,1)S(1)} %copy-done.2), kind=kOutput, calls=%fused_computation.15 | convolution fusion | flops 4031447040 | bytes 15269888 | tf_op jit(solution)/shard_map/sejd,edf->sejf/dot_general | solution.py:79
  116.3 0.5 copy.40
  116.9 1.5 collective-permute-start
  118.4 22.8 %collective-permute-done = bf16[8,1,60,1024]{3,0,2,1:T(8,128)(2,1)S(1)} collective-permute-done((bf16[8,1,60,1024]{3,0,2,1:T(8,128)(2,1)S(1)}, bf16[8,1,60,1024]{3,0,2,1:T(8,128)(2,1)S(1)}, u32[]{:S(2)}, u32[]{:S(2)}) %collective-permute-start) | collective-permute-done | bytes 983072 | tf_op jit(solution)/shard_map/ppermute | solution.py:16
  141.1 0.6 collective-permute-start.1
  141.7 22.8 %collective-permute-done.1 = bf16[8,1,60,1024]{3,0,2,1:T(8,128)(2,1)S(1)} collective-permute-done((bf16[8,1,60,1024]{3,0,2,1:T(8,128)(2,1)S(1)}, bf16[8,1,60,1024]{3,0,2,1:T(8,128)(2,1)S(1)}, u32[]{:S(2)}, u32[]{:S(2)}) %collective-permute-start.1) | collective-permute-done | bytes 983072 | tf_op jit(solution)/shard_map/ppermute | solution.py:16
  164.5 3.0 %fusion.12 = f32[1024,8,60]{0,2,1:T(8,128)S(1)} fusion(bf16[8,60,1024]{2,1,0:T(8,128)(2,1)S(1)} %multiply_convert_fusion, bf16[1,4096,1024]{2,1,0:T(8,128)(2,1)} %param.13, s32[]{:T(128)S(6)} %select_n.35), kind=kOutput, calls=%fused_computation.13 | convolution fusion | flops 1006632960 | bytes 5046276 | tf_op jit(solution)/shard_map/sejf,efd->sejd/dot_general | solution.py:49
  167.5 3.1 %fusion.10 = f32[1024,8,60]{0,2,1:T(8,128)S(1)} fusion(bf16[1,4096,1024]{2,1,0:T(8,128)(2,1)} %param.13, s32[]{:T(128)S(6)} %select_n.38, bf16[8,1,60,1024]{3,0,2,1:T(8,128)(2,1)S(1)} %collective-permute-done), kind=kOutput, calls=%fused_computation.11 | convolution fusion | flops 1006632960 | bytes 5046276 | tf_op jit(solution)/shard_map/sejf,efd->sejd/dot_general | solution.py:49
  170.7 1.4 fusion.8
  172.0 15.0 %collective-permute-done.2 = bf16[8,1,60,1024]{3,0,2,1:T(8,128)(2,1)S(1)} collective-permute-done((bf16[8,1,60,1024]{3,0,2,1:T(8,128)(2,1)S(1)}, bf16[8,1,60,1024]{3,0,2,1:T(8,128)(2,1)S(1)}, u32[]{:S(2)}, u32[]{:S(2)}) %collective-permute-start.2) | collective-permute-done | bytes 983072 | tf_op jit(solution)/shard_map/ppermute | solution.py:16
  187.0 2.4 %fusion.24 = bf16[8,1,60,1024]{3,2,1,0:T(8,128)(2,1)} fusion(bf16[1,4096,1024]{2,1,0:T(8,128)(2,1)S(1)} %bitcast.85, s32[]{:T(128)S(6)} %select_n.42, f32[1024,8,60]{0,2,1:T(8,128)S(1)} %fusion.8, f32[1024,8,60]{0,2,1:T(8,128)S(1)} %fusion.12, f32[1024,8,60]{0,2,1:T(8,128)S(1)} %fusion.10, bf16[8,1,60,1024]{3,0,2,1:T(8,128)(2,1)S(1)} %collective-permute-done.2), kind=kOutput, calls=%fused_computation.23 | convolution fusion | flops 1008599040 | bytes 10354692 | tf_op jit(solution)/shard_map/sejf,efd->sejd/dot_general | solution.py:49
  189.4 4.8 %all-to-all-start.1 = ((bf16[8,1,60,1024]{3,2,1,0:T(8,128)(2,1)}), bf16[8,1,60,1024]{3,2,1,0:T(8,128)(2,1)S(1)}, u32[]{:S(2)}, u32[]{:S(2)}) async-start(bf16[8,1,60,1024]{3,2,1,0:T(8,128)(2,1)} %fusion.24), calls=%async_computation.1 | async-start | bytes 2097152 | tf_op jit(solution)/shard_map/all_to_all | solution.py:82
  194.4 0.3 eq.65
  194.6 26.1 %all-to-all-done.1 = bf16[8,1,60,1024]{3,2,1,0:T(8,128)(2,1)S(1)} async-done(((bf16[8,1,60,1024]{3,2,1,0:T(8,128)(2,1)}), bf16[8,1,60,1024]{3,2,1,0:T(8,128)(2,1)S(1)}, u32[]{:S(2)}, u32[]{:S(2)}) %all-to-all-start.1) | async-done | bytes 983072 | tf_op jit(solution)/shard_map/all_to_all | solution.py:82
  220.9 1.4 multiply_reduce_fusion.1
  (33 shorter events, 1.4 us)
Async XLA Ops:
  6.5 92.2 %all-gather.2.cloned.1.call-start = ((), (), s32[]{:S(2)}) async-start(), calls=%async_computation.2 | async-start | bytes 5242880 | tf_op jit(solution)/shard_map/all_gather | solution.py:77
  6.5 1.9 copy-start
  6.5 2.3 copy-start.1
  98.8 9.1 %copy-start.2 = (bf16[8,1,60,4096]{3,2,0,1:T(8,128)(2,1)S(1)}, bf16[8,1,60,4096]{3,2,0,1:T(8,128)(2,1)}, u32[]{:S(2)}) copy-start(bf16[8,1,60,4096]{3,2,0,1:T(8,128)(2,1)} %all-gather.2.cloned.1.call-done) | copy-start | bytes 11796484
  116.9 24.3 %collective-permute-start = (bf16[8,1,60,1024]{3,0,2,1:T(8,128)(2,1)S(1)}, bf16[8,1,60,1024]{3,0,2,1:T(8,128)(2,1)S(1)}, u32[]{:S(2)}, u32[]{:S(2)}) collective-permute-start(bf16[8,1,60,1024]{3,0,2,1:T(8,128)(2,1)S(1)} %copy.40), channel_id=1, source_target_pairs={{0,1},{1,2},{2,3},{3,0},{4,5},{5,6},{6,7},{7,4},{8,9},{9,10},{10,1... | collective-permute-start | bytes 2949128 | tf_op jit(solution)/shard_map/ppermute | solution.py:16
  141.1 23.4 %collective-permute-start.1 = (bf16[8,1,60,1024]{3,0,2,1:T(8,128)(2,1)S(1)}, bf16[8,1,60,1024]{3,0,2,1:T(8,128)(2,1)S(1)}, u32[]{:S(2)}, u32[]{:S(2)}) collective-permute-start(bf16[8,1,60,1024]{3,0,2,1:T(8,128)(2,1)S(1)} %collective-permute-done), channel_id=1, source_target_pairs={{0,1},{1,2},{2,3},{3,0},{4,5},{5,6},{6,7},{7,4},{8,9},{9,10},{10,1... | collective-permute-start | bytes 2949128 | tf_op jit(solution)/shard_map/ppermute | solution.py:16
  164.5 22.5 %collective-permute-start.2 = (bf16[8,1,60,1024]{3,0,2,1:T(8,128)(2,1)S(1)}, bf16[8,1,60,1024]{3,0,2,1:T(8,128)(2,1)S(1)}, u32[]{:S(2)}, u32[]{:S(2)}) collective-permute-start(bf16[8,1,60,1024]{3,0,2,1:T(8,128)(2,1)S(1)} %collective-permute-done.1), channel_id=1, source_target_pairs={{0,1},{1,2},{2,3},{3,0},{4,5},{5,6},{6,7},{7,4},{8,9},{9,10},{10,1... | collective-permute-start | bytes 2949128 | tf_op jit(solution)/shard_map/ppermute | solution.py:16
  164.5 6.1 %slice-start = ((s8[8388608]{0:T(1024)(128)(4,1)}), s8[4194304]{0:T(1024)(128)(4,1)S(1)}, s32[]{:S(2)}) async-start(s8[8388608]{0:T(1024)(128)(4,1)} %bitcast.84), calls=%async_computation.3 | async-start | bytes 8388608
  167.5 3.1 %slice-start.1 = ((s8[8388608]{0:T(1024)(128)(4,1)}), s8[4194304]{0:T(1024)(128)(4,1)S(1)}, s32[]{:S(2)}) async-start(s8[8388608]{0:T(1024)(128)(4,1)} %bitcast.84), calls=%async_computation.4 | async-start | bytes 8388608
  189.4 31.5 %copy-start.3 = (f32[192,2]{0,1:T(2,128)S(1)}, f32[192,2]{0,1:T(2,128)}, u32[]{:S(2)}) copy-start(f32[192,2]{0,1:T(2,128)} %param.9) | copy-start | bytes 4612
  189.4 31.3 %all-to-all-start.1 = ((bf16[8,1,60,1024]{3,2,1,0:T(8,128)(2,1)}), bf16[8,1,60,1024]{3,2,1,0:T(8,128)(2,1)S(1)}, u32[]{:S(2)}, u32[]{:S(2)}) async-start(bf16[8,1,60,1024]{3,2,1,0:T(8,128)(2,1)} %fusion.24), calls=%async_computation.1 | async-start | bytes 2097152 | tf_op jit(solution)/shard_map/all_to_all | solution.py:82
Sparse Core Ops, SparseCore 0:
  47.2 51.4 all-gather.1
